TPU v7x, 32 devices: a whole 2x2x4 slice. The times are simulated.
32 devices in a mesh: sp: 4 (over z), fs: 4 (over y, x), tp: 2 (over core).
Axes of the slice: x: 2, y: 2, z: 4, core: 2. Of those that a mesh axis runs over, the one named last changes fastest.
Arguments:
- tokens: bfloat16 [4, 1536, 2048], P('fs', ('sp', 'tp')), may hold values from -6 to 6
- norm_gain: float32 [2048], replicated, may hold values from 0.1 to 1.9
- conv_gate_w: bfloat16 [2048, 1024], P('sp', 'tp'), may hold values from -0.125 to 0.125
- conv_in_w: bfloat16 [2048, 1024], P('sp', 'tp'), may hold values from -0.125 to 0.125
- query_w: bfloat16 [2048, 1024], P('sp', 'tp'), may hold values from -0.125 to 0.125
- forget_w: bfloat16 [2048, 1024], P('sp', 'tp'), may hold values from -0.125 to 0.125
- value_w: bfloat16 [2048, 1024], P('sp', 'tp'), may hold values from -0.125 to 0.125
- conv_taps: float32 [3, 1024], P(None, 'tp'), may hold values from -3.5 to 3.5
- floor_gate: float32 [1024], P('tp'), may hold values from 0.93 to 1
- leak: float32 [4, 1536, 8], P('fs', 'sp', 'tp'), may hold values from -1.4 to 0
- head_gain: float32 [128], replicated, may hold values from 0.1 to 1.9
- conv_out_w: bfloat16 [1024, 2048], P('tp', 'fs'), may hold values from -0.125 to 0.125
- chain_out_w: bfloat16 [1024, 2048], P('tp', 'fs'), may hold values from -0.125 to 0.125
Outputs:
- mixed: bfloat16 [4, 1536, 2048], P('fs', ('sp', 'tp'))
All inputs are finite; a program needn't handle non-finite values.
Results may differ from a plain program's by a relative error of at most 0.013.
Values may be sent and summed in bfloat16 or wider, within the bound.
A program may use at most 128 MiB of HBM per device.

v0:
```python
import jax
import jax.numpy as jnp
from jax import lax
from jax.sharding import PartitionSpec as P

BLOCK = 64


HIGH_ACCURACY = lax.Precision.HIGHEST


def as_sent(array):

    def short(part):
        return part.astype(jnp.bfloat16) if part.dtype == jnp.float32 else part

    return jax.tree.map(short, array)


def passed_along(array, axis, by):
    count = lax.axis_size(axis)
    pairs = [(i, i + by) for i in range(count) if 0 <= i + by < count]
    return lax.ppermute(array, axis, pairs)


def entering(value, axis, join, neutral):
    count, mine = (lax.axis_size(axis), lax.axis_index(axis))
    pieces = jax.tree.map(lambda part: lax.all_gather(part, axis), value)
    subtotal = jax.tree.map(
        lambda part, zero: jnp.full_like(part, 0) + jnp.asarray(zero, part.dtype), value, neutral
    )

    def hop(position, subtotal):
        longer = join(subtotal, jax.tree.map(lambda part: part[position], pieces))
        return jax.tree.map(lambda new, old: jnp.where(position < mine, new, old), longer, subtotal)

    return lax.fori_loop(0, count - 1, hop, subtotal)


def norm_rows(matrix, norm_gain):
    values = matrix.astype(jnp.float32)
    center = values - jnp.mean(values, axis=-1, keepdims=True)
    spread = jnp.mean(center * center, axis=-1, keepdims=True)
    return (center * lax.rsqrt(spread + 1e-05) * norm_gain).astype(jnp.bfloat16)


def block_chain(query, keys, values, decay):
    heads, length, width = query.shape
    count = length // BLOCK

    def split_blocks(array):
        return array.reshape(heads, count, BLOCK, array.shape[-1]).transpose(1, 0, 2, 3)

    causal = jnp.tril(jnp.ones((BLOCK, BLOCK), jnp.float32))

    def advance(hidden_state, inputs):
        query_part, key_portion, value_portion, decay_part = inputs
        running_state = jnp.cumsum(decay_part, axis=1)
        scaled_query = query_part * jnp.exp(running_state)
        key_scaled = key_portion * jnp.exp(-running_state)
        scores = (
            jnp.einsum("htk,hsk->hts", scaled_query, key_scaled, precision=HIGH_ACCURACY) * causal
        )
        inside = jnp.einsum("hts,hsv->htv", scores, value_portion, precision=HIGH_ACCURACY)
        carried_state = jnp.einsum(
            "rgn,rns->rgs", scaled_query, hidden_state, precision=HIGH_ACCURACY
        )
        final_state = running_state[:, -1:, :]
        state_update = jnp.einsum(
            "qdm,qdt->qmt",
            key_portion * jnp.exp(final_state - running_state),
            value_portion,
            precision=HIGH_ACCURACY,
        )
        return (
            jnp.exp(final_state[:, 0, :])[:, :, None] * hidden_state + state_update,
            inside + carried_state,
        )

    initial = jnp.zeros((heads, width, values.shape[-1]), jnp.float32)
    hidden_state, layer_results = lax.scan(
        advance,
        initial,
        (split_blocks(query), split_blocks(keys), split_blocks(values), split_blocks(decay)),
    )
    return (
        layer_results.transpose(1, 0, 2, 3).reshape(heads, length, values.shape[-1]),
        hidden_state,
    )


def chain_join(earlier_tokens, later):
    return (
        earlier_tokens[0] + later[0],
        jnp.exp(later[0])[:, :, None] * earlier_tokens[1] + later[1],
    )


def body(
    tokens,
    norm_gain,
    conv_gate_w,
    conv_in_w,
    query_w,
    forget_w,
    value_w,
    conv_taps,
    floor_gate,
    leak,
    head_gain,
    conv_out_w,
    chain_out_w,
):
    own_rows = norm_rows(tokens[0], norm_gain)
    normed = lax.all_gather(own_rows, "tp", axis=0, tiled=True)
    length = normed.shape[0]
    weights = (conv_gate_w, conv_in_w, query_w, forget_w, value_w)
    groups = lax.axis_size("fs")
    member = lax.axis_index("fs")
    sliced = tuple(
        (
            lax.dynamic_slice_in_dim(
                weight, member * (weight.shape[1] // groups), weight.shape[1] // groups, 1
            )
            for weight in weights
        )
    )
    pooled = lax.all_gather(normed[None], "fs", axis=0, tiled=True)
    flat_rows = pooled.reshape(groups * length, pooled.shape[2])
    pieces = jax.tree.map(
        lambda part: lax.all_gather(part, "sp", axis=0, tiled=True), as_sent(sliced)
    )
    sums = tuple(
        (jnp.dot(flat_rows, piece, preferred_element_type=jnp.float32) for piece in pieces)
    )
    quarters = tuple(
        (total.astype(jnp.bfloat16).reshape(groups, length, total.shape[1]) for total in sums)
    )
    returned = jax.tree.map(
        lambda part, own: part.astype(own.dtype),
        lax.all_to_all(as_sent(quarters), "fs", split_axis=0, concat_axis=2, tiled=True),
        quarters,
    )
    projected = tuple((column_set[0] for column_set in returned))
    second_gate, signal, query_raw, forget_raw, value_raw = projected
    margin = conv_taps.shape[0] - 1
    rim = passed_along(signal[length - margin :], "sp", 1)
    padded = jnp.concatenate([rim, signal], axis=0).astype(jnp.float32)
    filtered = jnp.zeros((length, signal.shape[1]), jnp.float32)
    for offset in range(margin + 1):
        filtered = filtered + conv_taps[offset] * padded[offset : offset + length]
    conv_mix = (second_gate.astype(jnp.float32) * filtered).astype(jnp.bfloat16)
    heads_here = leak.shape[2]
    head_width = query_raw.shape[1] // heads_here

    def by_head(array):
        return array.astype(jnp.float32).reshape(length, heads_here, head_width).transpose(1, 0, 2)

    floor = floor_gate.reshape(heads_here, 1, head_width)
    logits = by_head(forget_raw)
    retain = floor + (1.0 - floor) * jax.nn.sigmoid(logits)
    keys = (1.0 - floor) * jax.nn.sigmoid(-logits)
    decay = jnp.log(retain) + leak[0].T[:, :, None]
    query = jax.nn.silu(by_head(query_raw))
    pairwise_dot, hidden_state = block_chain(query, keys, by_head(value_raw), decay)
    total_decay = jnp.sum(decay, axis=1)
    identity = (jnp.zeros_like(total_decay), jnp.zeros_like(hidden_state))
    earlier_tokens = entering((total_decay, hidden_state), "sp", chain_join, identity)
    filter_reach = query * jnp.exp(jnp.cumsum(decay, axis=1))
    recurrence_raw = pairwise_dot + jnp.einsum(
        "rgn,rns->rgs", filter_reach, earlier_tokens[1], precision=HIGH_ACCURACY
    )
    scale = lax.rsqrt(jnp.mean(recurrence_raw * recurrence_raw, axis=-1, keepdims=True) + 1e-06)
    chain_mix = (
        (recurrence_raw * scale * head_gain)
        .transpose(1, 0, 2)
        .reshape(length, heads_here * head_width)
        .astype(jnp.bfloat16)
    )
    conv_full, chain_full = (
        lax.all_gather(conv_out_w, "fs", axis=1, tiled=True),
        lax.all_gather(chain_out_w, "fs", axis=1, tiled=True),
    )
    mixed = lax.psum_scatter(
        jnp.dot(conv_mix, conv_full, preferred_element_type=jnp.float32)
        + jnp.dot(chain_mix, chain_full, preferred_element_type=jnp.float32),
        "tp",
        scatter_dimension=0,
        tiled=True,
    )
    return mixed.astype(jnp.bfloat16)[None]


def solution(mesh):
    in_specs = (
        P("fs", ("sp", "tp"), None),
        P(),
        P("sp", "tp"),
        P("sp", "tp"),
        P("sp", "tp"),
        P("sp", "tp"),
        P("sp", "tp"),
        P(None, "tp"),
        P("tp"),
        P("fs", "sp", "tp"),
        P(),
        P("tp", "fs"),
        P("tp", "fs"),
    )
    out_specs = P("fs", ("sp", "tp"), None)
    return jax.shard_map(body, mesh=mesh, in_specs=in_specs, out_specs=out_specs, check_vma=False)
```

profile of v0, /device:TPU:0, one launch (start us, length us, event | category | flops | bytes accessed | tf_op | source)
XLA Modules:
  0.0 289.1 jit_solution(1176081124464315372)
XLA Ops:
  11.6 12.6 %all-gather.10.cloned.1.call-done = bf16[384,2048]{1,0:T(8,128)(2,1)} async-done(((bf16[192,2048]{1,0:T(8,128)(2,1)}), bf16[384,2048]{1,0:T(8,128)(2,1)}) %all-gather.10.cloned.1.call-update) | async-done | bytes 1572880 | tf_op jit(solution)/shard_map/all_gather | solution.py:115
  25.0 16.3 %all_gather.44 = bf16[2048,128]{1,0:T(8,128)(2,1)S(1)} all-gather(bf16[512,128]{1,0:T(8,128)(2,1)S(1)} %constant_dynamic-slice_fusion.2), channel_id=1, replica_groups=mesh['sp'=4,'fs'=4,'tp'=2] {'sp'}, dimensions={0}, use_global_device_ids=true | all-gather | bytes 655360 | tf_op jit(solution)/shard_map/all_gather | solution.py:131
  42.3 16.1 %all_gather.46 = bf16[2048,128]{1,0:T(8,128)(2,1)S(1)} all-gather(bf16[512,128]{1,0:T(8,128)(2,1)S(1)} %constant_dynamic-slice_fusion), channel_id=1, replica_groups=mesh['sp'=4,'fs'=4,'tp'=2] {'sp'}, dimensions={0}, use_global_device_ids=true | all-gather | bytes 655360 | tf_op jit(solution)/shard_map/all_gather | solution.py:131
  59.3 15.8 %all_gather.45 = bf16[2048,128]{1,0:T(8,128)(2,1)S(1)} all-gather(bf16[512,128]{1,0:T(8,128)(2,1)S(1)} %constant_dynamic-slice_fusion.1), channel_id=1, replica_groups=mesh['sp'=4,'fs'=4,'tp'=2] {'sp'}, dimensions={0}, use_global_device_ids=true | all-gather | bytes 655360 | tf_op jit(solution)/shard_map/all_gather | solution.py:131
  75.1 22.2 %all-gather.16.cloned.1.call-done = bf16[1536,2048]{1,0:T(8,128)(2,1)} async-done(((bf16[384,2048]{1,0:T(8,128)(2,1)}), bf16[1536,2048]{1,0:T(8,128)(2,1)}) %all-gather.16.cloned.1.call-update) | async-done | bytes 6291472 | tf_op jit(solution)/shard_map/all_gather | solution.py:128
  97.3 5.4 %convolution_convert_fusion.2 = bf16[1536,128]{1,0:T(8,128)(2,1)} fusion(bf16[1536,2048]{1,0:T(8,128)(2,1)} %all-gather.16.cloned.1.call-done, bf16[2048,128]{1,0:T(8,128)(2,1)S(1)} %all_gather.44), kind=kOutput, calls=%fused_computation.38 | convolution fusion | flops 805502976 | bytes 7208960 | tf_op jit(solution)/shard_map/dot_general | solution.py:134
  102.6 3.5 %all-to-all-start.2 = ((bf16[4,384,128]{2,1,0:T(8,128)(2,1)}), bf16[4,384,128]{2,1,0:T(8,128)(2,1)S(1)}, u32[]{:S(2)}, u32[]{:S(2)}) async-start(bf16[4,384,128]{2,1,0:T(8,128)(2,1)} %bitcast.15), calls=%async_computation.2 | async-start | bytes 786432 | tf_op jit(solution)/shard_map/all_to_all | solution.py:141
  106.1 5.7 %convolution_convert_fusion = bf16[1536,128]{1,0:T(8,128)(2,1)} fusion(bf16[1536,2048]{1,0:T(8,128)(2,1)} %all-gather.16.cloned.1.call-done, bf16[2048,128]{1,0:T(8,128)(2,1)S(1)} %all_gather.46), kind=kOutput, calls=%fused_computation.36 | convolution fusion | flops 805502976 | bytes 7208960 | tf_op jit(solution)/shard_map/dot_general | solution.py:134
  117.1 3.5 %all-to-all-start.3 = ((bf16[4,384,128]{2,1,0:T(8,128)(2,1)}), bf16[4,384,128]{2,1,0:T(8,128)(2,1)S(1)}, u32[]{:S(2)}, u32[]{:S(2)}) async-start(bf16[4,384,128]{2,1,0:T(8,128)(2,1)} %bitcast.30), calls=%async_computation.3 | async-start | bytes 786432 | tf_op jit(solution)/shard_map/all_to_all | solution.py:141
  127.2 3.5 %all-to-all-start.4 = ((bf16[4,384,128]{2,1,0:T(8,128)(2,1)}), bf16[4,384,128]{2,1,0:T(8,128)(2,1)S(1)}, u32[]{:S(2)}, u32[]{:S(2)}) async-start(bf16[4,384,128]{2,1,0:T(8,128)(2,1)} %bitcast.33), calls=%async_computation.4 | async-start | bytes 786432 | tf_op jit(solution)/shard_map/all_to_all | solution.py:141
  134.8 6.2 %all-to-all-done.4 = bf16[4,384,128]{2,1,0:T(8,128)(2,1)S(1)} async-done(((bf16[4,384,128]{2,1,0:T(8,128)(2,1)}), bf16[4,384,128]{2,1,0:T(8,128)(2,1)S(1)}, u32[]{:S(2)}, u32[]{:S(2)}) %all-to-all-start.4) | async-done | bytes 393248 | tf_op jit(solution)/shard_map/all_to_all | solution.py:141
  143.3 20.6 %while.27 = (s32[]{:T(128)}, f32[4,128,128]{2,1,0:T(8,128)S(1)}, f32[6,4,64,128]{3,2,0,1:T(8,128)}, f32[6,4,64,128]{3,2,0,1:T(8,128)}, f32[6,4,64,128]{3,2,0,1:T...) while((s32[]{:T(128)}, f32[4,128,128]{2,1,0:T(8,128)S(1)}, ...), condition=%wide.region_4.5_spmd.clone, body=%wide.region_2.4_spmd.clone.sunk | while | flops 153575424 | bytes 3275900 | solution.py:81
  166.5 21.4 %all_gather.42 = bf16[2048,128]{1,0:T(8,128)(2,1)S(1)} all-gather(bf16[512,128]{1,0:T(8,128)(2,1)S(1)} %constant_dynamic-slice_fusion.3), channel_id=1, replica_groups=mesh['sp'=4,'fs'=4,'tp'=2] {'sp'}, dimensions={0}, use_global_device_ids=true | all-gather | bytes 655360 | tf_op jit(solution)/shard_map/all_gather | solution.py:131
  187.9 18.9 %all_gather.41 = bf16[2048,128]{1,0:T(8,128)(2,1)S(1)} all-gather(bf16[512,128]{1,0:T(8,128)(2,1)S(1)} %constant_dynamic-slice_fusion.4), channel_id=1, replica_groups=mesh['sp'=4,'fs'=4,'tp'=2] {'sp'}, dimensions={0}, use_global_device_ids=true | all-gather | bytes 655360 | tf_op jit(solution)/shard_map/all_gather | solution.py:131
  206.9 4.6 %convolution_convert_fusion.3 = bf16[1536,128]{1,0:T(8,128)(2,1)S(1)} fusion(bf16[1536,2048]{1,0:T(8,128)(2,1)} %all-gather.16.cloned.1.call-done, bf16[2048,128]{1,0:T(8,128)(2,1)S(1)} %all_gather.42), kind=kOutput, calls=%fused_computation.39 | convolution fusion | flops 805502976 | bytes 7208960 | tf_op jit(solution)/shard_map/dot_general | solution.py:134
  212.4 3.5 %all-to-all-start.1 = ((bf16[4,384,128]{1,2,0:T(8,128)(2,1)}), bf16[4,384,128]{1,2,0:T(8,128)(2,1)S(1)}, u32[]{:S(2)}, u32[]{:S(2)}) async-start(bf16[4,384,128]{1,2,0:T(8,128)(2,1)} %copy.28), calls=%async_computation.1 | async-start | bytes 786432 | tf_op jit(solution)/shard_map/all_to_all | solution.py:141
  215.9 4.6 %convolution_convert_fusion.4 = bf16[1536,128]{1,0:T(8,128)(2,1)S(1)} fusion(bf16[1536,2048]{1,0:T(8,128)(2,1)} %all-gather.16.cloned.1.call-done, bf16[2048,128]{1,0:T(8,128)(2,1)S(1)} %all_gather.41), kind=kOutput, calls=%fused_computation.40 | convolution fusion | flops 805502976 | bytes 7208960 | tf_op jit(solution)/shard_map/dot_general | solution.py:134
  221.7 3.9 %all-to-all-start = ((bf16[4,384,128]{1,2,0:T(8,128)(2,1)}), bf16[4,384,128]{1,2,0:T(8,128)(2,1)S(1)}, u32[]{:S(2)}, u32[]{:S(2)}) async-start(bf16[4,384,128]{1,2,0:T(8,128)(2,1)} %copy.27), calls=%async_computation | async-start | bytes 786432 | tf_op jit(solution)/shard_map/all_to_all | solution.py:141
  231.5 11.9 %all-gather.3 = f32[4,4,128]{2,1,0:T(4,128)S(1)} all-gather(f32[1,4,128]{2,1,0:T(4,128)S(1)} %bitcast.201), channel_id=3, replica_groups=mesh['sp'=4,'fs'=4,'tp'=2] {'sp'}, dimensions={0}, use_global_device_ids=true | all-gather | bytes 10240 | tf_op jit(solution)/shard_map/all_gather | solution.py:28
  244.5 4.2 %fusion.54 = f32[384,2048]{1,0:T(8,128)} fusion(bf16[384,512]{0,1:T(8,128)(2,1)S(1)} %fusion.50, bf16[512,2048]{1,0:T(8,128)(2,1)} %all-gather.12.cloned.1.call-done), kind=kOutput, calls=%fused_computation.99 | convolution fusion | flops 805306368 | bytes 5636096 | tf_op jit(solution)/shard_map/dot_general | solution.py:185
  248.8 3.7 %while.28 = (s32[]{:T(128)}, f32[4,128,128]{2,1,0:T(8,128)S(1)}, s32[]{:T(128)}, f32[4,4,128]{2,1,0:T(4,128)S(1)}, f32[4,4,128,128]{3,2,1,0:T(8,128)}, /*index=5*/s32[]{:T(128)}, s32[]{:T(128)}) while((s32[]{:T(128)}, f32[4,128,128]{2,1,0:T(8,128)S(1)}, s32[]{:T(128)}, f32[4,4,128]{2,1,0:T(4,128)S(1)}, ...), condition=%wide.region_9.10_spmd.clone, body=%wide.region_8.9_spmd.clone.sunk | while | flops 262148 | bytes 792681 | solution.py:37
  253.8 9.6 %all-gather.14.cloned.1.call-done = bf16[512,2048]{1,0:T(8,128)(2,1)} async-done(((bf16[512,512]{1,0:T(8,128)(2,1)}), bf16[512,2048]{1,0:T(8,128)(2,1)}) %all-gather.14.cloned.1.call-update) | async-done | bytes 2097168 | tf_op jit(solution)/shard_map/all_gather | solution.py:182
  263.3 5.2 %convolution_add_fusion.2 = f32[384,2048]{1,0:T(8,128)} fusion(f32[384,2048]{1,0:T(8,128)} %fusion.54, bf16[384,512]{0,1:T(8,128)(2,1)S(1)} %bitcast.187, bf16[512,2048]{1,0:T(8,128)(2,1)} %all-gather.14.cloned.1.call-done), kind=kOutput, calls=%fused_computation.35 | convolution fusion | flops 806092800 | bytes 8781824 | tf_op jit(solution)/shard_map/dot_general | solution.py:186
  268.5 11.3 %reduce-scatter.2.cloned.1.call-done = f32[192,2048]{1,0:T(8,128)} async-done(((f32[384,2048]{1,0:T(8,128)}), f32[192,2048]{1,0:T(8,128)}) %reduce-scatter.2.cloned.1.call-update) | async-done | bytes 1572880 | tf_op jit(solution)/shard_map/reduce_scatter | solution.py:184
  (141 shorter events, 65.1 us)
Async XLA Ops:
  6.5 18.4 %copy-start = (bf16[512,512]{1,0:T(8,128)(2,1)S(1)}, bf16[512,512]{1,0:T(8,128)(2,1)}, u32[]{:S(2)}) copy-start(bf16[512,512]{1,0:T(8,128)(2,1)} %param.22) | copy-start | bytes 1572868
  6.5 2.9 %copy-start.2 = (bf16[1,192,2048]{2,1,0:T(8,128)(2,1)S(1)}, bf16[1,192,2048]{2,1,0:T(8,128)(2,1)}, u32[]{:S(2)}) copy-start(bf16[1,192,2048]{2,1,0:T(8,128)(2,1)} %param.17) | copy-start | bytes 2359300
  6.5 17.7 %all-gather.10.cloned.1.call-start = ((), (), s32[]{:S(2)}) async-start(), calls=%async_computation.6 | async-start | bytes 2359296 | tf_op jit(solution)/shard_map/all_gather | solution.py:115
  11.5 29.9 %copy-start.7 = (f32[512]{0:T(512)S(1)}, f32[512]{0:T(512)}, u32[]{:S(2)}) copy-start(f32[512]{0:T(512)} %param.25) | copy-start | bytes 6148
  11.5 85.8 %all-gather.16.cloned.1.call-start = ((), (), s32[]{:S(2)}) async-start(), calls=%async_computation.10 | async-start | bytes 7864320 | tf_op jit(solution)/shard_map/all_gather | solution.py:128
  24.2 220.3 %all-gather.12.cloned.1.call-start = ((), (), s32[]{:S(2)}) async-start(), calls=%async_computation.7 | async-start | bytes 2621440 | tf_op jit(solution)/shard_map/all_gather | solution.py:181
  102.6 14.4 %all-to-all-start.2 = ((bf16[4,384,128]{2,1,0:T(8,128)(2,1)}), bf16[4,384,128]{2,1,0:T(8,128)(2,1)S(1)}, u32[]{:S(2)}, u32[]{:S(2)}) async-start(bf16[4,384,128]{2,1,0:T(8,128)(2,1)} %bitcast.15), calls=%async_computation.2 | async-start | bytes 786432 | tf_op jit(solution)/shard_map/all_to_all | solution.py:141
  106.1 5.7 %copy-start.11 = (bf16[1536,2048]{1,0:T(8,128)(2,1)S(1)}, bf16[1536,2048]{1,0:T(8,128)(2,1)}, u32[]{:S(2)}) copy-start(bf16[1536,2048]{1,0:T(8,128)(2,1)} %all-gather.16.cloned.1.call-done) | copy-start | bytes 18874372
  111.8 8.7 %copy-start.6 = (f32[1,384,4]{1,2,0:T(4,128)S(1)}, f32[1,384,4]{1,2,0:T(4,128)}, u32[]{:S(2)}) copy-start(f32[1,384,4]{1,2,0:T(4,128)} %param.26) | copy-start | bytes 18436
  117.1 10.1 %all-to-all-start.3 = ((bf16[4,384,128]{2,1,0:T(8,128)(2,1)}), bf16[4,384,128]{2,1,0:T(8,128)(2,1)S(1)}, u32[]{:S(2)}, u32[]{:S(2)}) async-start(bf16[4,384,128]{2,1,0:T(8,128)(2,1)} %bitcast.30), calls=%async_computation.3 | async-start | bytes 786432 | tf_op jit(solution)/shard_map/all_to_all | solution.py:141
  121.4 1.0 copy-start.3
  127.2 13.9 %all-to-all-start.4 = ((bf16[4,384,128]{2,1,0:T(8,128)(2,1)}), bf16[4,384,128]{2,1,0:T(8,128)(2,1)S(1)}, u32[]{:S(2)}, u32[]{:S(2)}) async-start(bf16[4,384,128]{2,1,0:T(8,128)(2,1)} %bitcast.33), calls=%async_computation.4 | async-start | bytes 786432 | tf_op jit(solution)/shard_map/all_to_all | solution.py:141
  130.7 118.1 %all-gather.18.cloned.1.call-start = ((), (), s32[]{:S(2)}) async-start(), calls=%async_computation.11 | async-start | bytes 1310720 | tf_op jit(solution)/shard_map/all_gather | solution.py:28
  163.9 0.7 copy-start.1
  212.4 9.3 %all-to-all-start.1 = ((bf16[4,384,128]{1,2,0:T(8,128)(2,1)}), bf16[4,384,128]{1,2,0:T(8,128)(2,1)S(1)}, u32[]{:S(2)}, u32[]{:S(2)}) async-start(bf16[4,384,128]{1,2,0:T(8,128)(2,1)} %copy.28), calls=%async_computation.1 | async-start | bytes 786432 | tf_op jit(solution)/shard_map/all_to_all | solution.py:141
  220.4 5.8 %copy-start.9 = (f32[3,512]{1,0:T(4,128)S(1)}, f32[3,512]{1,0:T(4,128)}, u32[]{:S(2)}) copy-start(f32[3,512]{1,0:T(4,128)} %param.24) | copy-start | bytes 18436
  220.5 5.8 %copy-start.5 = (f32[6,4,64,128]{3,2,0,1:T(8,128)S(1)}, f32[6,4,64,128]{3,2,0,1:T(8,128)}, u32[]{:S(2)}) copy-start(f32[6,4,64,128]{3,2,0,1:T(8,128)} %get-tuple-element.142) | copy-start | bytes 2359300
  221.4 10.1 %copy-start.8 = (f32[4,128]{1,0:T(4,128)S(1)}, f32[4,128]{1,0:T(4,128)}, u32[]{:S(2)}) copy-start(f32[4,128]{1,0:T(4,128)} %get-tuple-element.227) | copy-start | bytes 6148
  221.7 9.7 %all-to-all-start = ((bf16[4,384,128]{1,2,0:T(8,128)(2,1)}), bf16[4,384,128]{1,2,0:T(8,128)(2,1)S(1)}, u32[]{:S(2)}, u32[]{:S(2)}) async-start(bf16[4,384,128]{1,2,0:T(8,128)(2,1)} %copy.27), calls=%async_computation | async-start | bytes 786432 | tf_op jit(solution)/shard_map/all_to_all | solution.py:141
  225.6 37.8 %all-gather.14.cloned.1.call-start = ((), (), s32[]{:S(2)}) async-start(), calls=%async_computation.8 | async-start | bytes 2621440 | tf_op jit(solution)/shard_map/all_gather | solution.py:182
  226.1 53.7 %reduce-scatter.2.cloned.1.call-start = ((), (), s32[]{:S(2)}) async-start(), calls=%async_computation.9 | async-start | bytes 4718592 | tf_op jit(solution)/shard_map/reduce_scatter | solution.py:184
  226.6 16.8 %collective-permute-start = (bf16[2,512]{0,1:T(8,128)(2,1)S(1)}, bf16[2,512]{0,1:T(8,128)(2,1)S(1)}, u32[]{:S(2)}, u32[]{:S(2)}) collective-permute-start(bf16[2,512]{0,1:T(8,128)(2,1)S(1)} %bitcast.195), channel_id=1, source_target_pairs={{0,8},{8,16},{16,24},{1,9},{9,17},{17,25},{2,10},{10,18},{18,26},{... | collective-permute-start | bytes 6152 | tf_op jit(solution)/shard_map/ppermute | solution.py:23
  248.8 3.7 %copy-start.4 = (f32[4,384,128]{2,1,0:T(8,128)S(1)}, f32[4,384,128]{2,1,0:T(8,128)}, u32[]{:S(2)}) copy-start(f32[4,384,128]{2,1,0:T(8,128)} %get-tuple-element.229) | copy-start | bytes 2359300
  252.4 1.2 copy-start.10
Sparse Core Ops, SparseCore 0:
  11.6 12.5 all-gather.9
  26.0 71.1 all-gather.15
  99.1 42.9 all-gather.11
  164.8 37.6 all-gather.17
  227.9 35.3 all-gather.13
  268.6 11.1 reduce-scatter.1
where the time goes:
time: 290 us; the launch traced here: 289 us
  blocking collectives  101 us (35%)
  waiting for transfers between devices  71 us (24%)
  matrix products  47.2 us (16%)
  other arithmetic  20.8 us (7%)
  starting transfers between devices  20.1 us (7%)
  local copies, waits for them, and re-layouts  15.3 us (5%)
  between operations  13.8 us (5%)
    all_gather x5, blocking collectives, body(): lax.all_gather(part, 'sp', axis=0, tiled=True)  88.6 us
    dot_general x5, matrix products, body(): jnp.dot(flat_rows, piece, preferred_element_type=jnp.float32)  22.8 us
    all_gather x1, waiting for transfers between devices, body(): pooled = lax.all_gather(normed[None], 'fs', axis=0, tiled=True)  22.2 us
    all_to_all x5, starting transfers between devices, body(): lax.all_to_all(as_sent(quarters), 'fs', split_axis=0, concat_axis=2, tile...  17.7 us
    all_to_all x5, waiting for transfers between devices, body(): lax.all_to_all(as_sent(quarters), 'fs', split_axis=0, concat_axis=2, tile...  14 us
    all_gather x1, waiting for transfers between devices, body(): normed = lax.all_gather(own_rows, 'tp', axis=0, tiled=True)  12.6 us
    all_gather x1, blocking collectives, entering(): pieces = jax.tree.map(lambda part: lax.all_gather(part, axis), value)  11.9 us
    reduce_scatter x1, waiting for transfers between devices, body(): lax.psum_scatter(jnp.dot(conv_mix, conv_full, preferred_element_type=jnp....  11.3 us
  transfers between devices with their start and end apart: 12, of which 9 were waited for; matrix products, arithmetic and copies ran while one was open for 24% of the time, Pallas kernels for 0%

commit v1 on v0

v1 whole, which is shorter than its diff:
```python
import functools

import jax
import jax.numpy as jnp
from jax import lax
from jax.experimental import pallas as pl
from jax.experimental.pallas import tpu as pltpu
from jax.sharding import PartitionSpec as P

MESH = pl.DeviceIdType.MESH
BF = jnp.bfloat16
F32 = jnp.float32
NT = (((1,), (1,)), ((), ()))
TN = (((0,), (0,)), ((), ()))
GATE, SIGNAL, QUERY, FORGET, VALUE = 4, 3, 1, 0, 2


def kernel(
    ns, nf,
    tok, gain, w0, w1, w2, w3, w4, taps, floor, leak, leak_t, hgain, cow, how,
    out,
    rows, wg, psend, prev, wo, rim, inside, reach, states, sdecay, sin, sout,
    lcol, lrow, mix, osend, orecv,
    zs, zsl, zr, zloc, rs, rr, ts, tr, ps, pr, os_, or_, oloc, ms, mr, ss, sr, es, er,
):
    s, f, t = lax.axis_index("sp"), lax.axis_index("fs"), lax.axis_index("tp")
    other = 1 - t
    half = tok.shape[1]
    length = 2 * half
    kd = w0.shape[0]
    wide = w0.shape[1] // nf
    ws = (w3, w2, w4, w1, w0)
    np_ = len(ws)
    has_left, has_right = s > 0, s < ns - 1

    barrier = pltpu.get_barrier_semaphore()
    pl.semaphore_signal(barrier, inc=1, device_id={"tp": other}, device_id_type=MESH)
    for d in range(1, nf):
        pl.semaphore_signal(barrier, inc=1, device_id={"fs": f ^ d}, device_id_type=MESH)

    @pl.when(has_left)
    def _():
        pl.semaphore_signal(barrier, inc=1, device_id={"sp": s - 1}, device_id_type=MESH)

    @pl.when(has_right)
    def _():
        pl.semaphore_signal(barrier, inc=1, device_id={"sp": s + 1}, device_id_type=MESH)

    ends = jnp.where(has_left, 1, 0) + jnp.where(has_right, 1, 0)
    pl.semaphore_wait(barrier, nf + ends)

    def remote(src, dst, send, recv, **where):
        return pltpu.make_async_remote_copy(
            src_ref=src, dst_ref=dst, send_sem=send, recv_sem=recv,
            device_id=where, device_id_type=MESH,
        )

    def wblock(b, p):
        return wg.at[p, pl.ds(pl.multiple_of(b * kd, kd), kd), :]

    def wown(p):
        return ws[p].at[:, pl.ds(pl.multiple_of(f * wide, wide), wide)]

    def own_right(p):
        return remote(wown(p), wblock(s, p), zs.at[s, p], zr.at[s, p], sp=s + 1)

    def own_left(p):
        return remote(wown(p), wblock(s, p), zsl.at[p], zr.at[s, p], sp=s - 1)

    def relay(b, p, to):
        return remote(wblock(b, p), wblock(b, p), zs.at[b, p], zr.at[b, p], sp=to)

    def send_own(p):
        @pl.when(has_right)
        def _():
            own_right(p).start()

        @pl.when(has_left)
        def _():
            own_left(p).start()

        pltpu.make_async_copy(wown(p), wblock(s, p), zloc.at[p]).start()

    def zrelay(p):
        def hop(k, carry):
            @pl.when(s - k >= 0)
            def _():
                relay(s - k, p, s + 1).wait_recv()

                @pl.when(has_right)
                def _():
                    relay(s - k, p, s + 1).start()

            @pl.when(s + k < ns)
            def _():
                relay(s + k, p, s - 1).wait_recv()

                @pl.when(has_left)
                def _():
                    relay(s + k, p, s - 1).start()

            return carry

        lax.fori_loop(1, ns, hop, 0)
        pltpu.make_async_copy(wown(p), wblock(s, p), zloc.at[p]).wait()
        if p + 2 < np_:
            send_own(p + 2)

    send_own(0)
    send_own(1)

    x = tok[0].astype(F32)
    center = x - jnp.mean(x, axis=-1, keepdims=True)
    spread = jnp.mean(center * center, axis=-1, keepdims=True)
    rows[f, t] = (center * lax.rsqrt(spread + 1e-05) * gain[...]).astype(BF)

    quarter = half // 2

    def piece(g, j):
        return rows.at[g, t, pl.ds(j * quarter, quarter), :]

    def row_copy(g, j, to, slot):
        return remote(piece(g, j), piece(g, j), rs.at[slot], rr.at[g ^ f ^ to, j], fs=to)

    def row_arrived(d, j):
        g = f ^ d
        remote(piece(g, j), piece(g, j), rs.at[0], rr.at[d, j], fs=f ^ 1).wait_recv()

    def row_send(d, j, to_d, slot):
        g = f ^ d
        to = f ^ to_d
        return remote(piece(g, j), piece(g, j), rs.at[slot], rr.at[d ^ to_d, j], fs=to)

    def twin(d):
        g = f ^ d
        return remote(rows.at[g, t], rows.at[g, t], ts.at[d], tr.at[d], tp=other)

    def twin_arrived(d):
        g = f ^ d
        remote(rows.at[g, other], rows.at[g, other], ts.at[d], tr.at[d], tp=other).wait_recv()

    row_send(0, 0, 1, 0).start()
    row_send(0, 1, 2, 1).start()
    row_send(0, 1, 1, 2).start()
    row_send(0, 0, 2, 3).start()
    twin(0).start()

    ri = lax.broadcasted_iota(jnp.int32, (length, length), 0)
    ci = lax.broadcasted_iota(jnp.int32, (length, length), 1)
    tril = (ri >= ci).astype(F32)
    triu = (ri <= ci).astype(F32)
    high = lax.Precision.HIGHEST
    heads = leak.shape[2]
    lsum = jnp.dot(tril, leak[0], precision=high, preferred_element_type=F32)
    lsum_t = jnp.dot(leak_t[...], triu, precision=high, preferred_element_type=F32)
    for h in range(heads):
        lcol[h] = jnp.broadcast_to(lsum[:, h : h + 1], (length, wide))
        lrow[h] = jnp.broadcast_to(lsum_t[h : h + 1, :], (8, length))

    zrelay(0)
    row_arrived(1, 0)
    row_send(1, 0, 2, 4).start()
    row_arrived(2, 1)
    row_send(2, 1, 1, 5).start()
    zrelay(1)
    row_arrived(1, 1)
    twin(1).start()
    row_arrived(2, 0)
    twin(2).start()
    zrelay(2)
    row_arrived(3, 0)
    row_arrived(3, 1)
    twin(3).start()
    for d in range(nf):
        twin_arrived(d)

    def project(p):
        def one(g, carry):
            lhs = jnp.concatenate([rows[g, 0], rows[g, 1]], axis=0)
            psend[g, p] = jnp.dot(lhs, wg[p], preferred_element_type=F32).astype(BF)
            return carry

        lax.fori_loop(0, nf, one, 0)
        for d in range(1, nf):
            returned(d, p).start()
        prev[f, p] = psend[f, p]

    def returned(d, p):
        g = f ^ d
        return remote(psend.at[g, p], prev.at[f, p], ps.at[d, p], pr.at[d, p], fs=g)

    def returned_arrived(d, p):
        g = f ^ d
        remote(psend.at[g, p], prev.at[g, p], ps.at[d, p], pr.at[d, p], fs=g).wait_recv()

    project(0)
    project(1)
    project(2)
    zrelay(3)
    project(3)
    zrelay(4)
    project(4)

    outs = (cow, how)

    def own_out(j, to_d, slot):
        return remote(outs[j], wo.at[f, j], os_.at[slot], or_.at[to_d, j], fs=f ^ to_d)

    def relay_out(d, j, to_d, slot):
        g = f ^ d
        return remote(wo.at[g, j], wo.at[g, j], os_.at[slot], or_.at[d ^ to_d, j], fs=f ^ to_d)

    def out_arrived(d, j):
        g = f ^ d
        remote(wo.at[g, j], wo.at[g, j], os_.at[0], or_.at[d, j], fs=f ^ 1).wait_recv()

    own_out(0, 1, 0).start()
    own_out(1, 2, 1).start()
    own_out(1, 1, 2).start()
    own_out(0, 2, 3).start()
    for j in range(2):
        pltpu.make_async_copy(outs[j], wo.at[f, j], oloc.at[j]).start()

    for p in range(3):
        for d in range(1, nf):
            returned_arrived(d, p)
    causal = ri >= ci

    def local(h, carry):
        fl = floor[h]
        logits = prev[h, FORGET].astype(F32)
        retain = fl + (1.0 - fl) * jax.nn.sigmoid(logits)
        keys = (1.0 - fl) * jax.nn.sigmoid(-logits)
        total = jnp.dot(tril, jnp.log(retain), precision=high, preferred_element_type=F32)
        raw = prev[h, QUERY].astype(F32)
        query = raw * jax.nn.sigmoid(raw) * jnp.exp(total)
        value = prev[h, VALUE]
        scores = lax.dot_general(
            query.astype(BF), (keys * jnp.exp(-total)).astype(BF), NT, preferred_element_type=F32
        )
        lc = lcol[h]
        gap = lc[:, 0:1] - lrow[h, 0:1, :]
        scores = jnp.where(causal, scores * jnp.exp(jnp.where(causal, gap, 0.0)), 0.0)
        inside[h] = jnp.dot(scores.astype(BF), value, preferred_element_type=F32)
        reach[h] = (query * jnp.exp(lc)).astype(BF)
        full = total + lc
        end = full[length - 1 :, :]
        update = (keys * jnp.exp(end - full)).astype(BF)
        states[h] = lax.dot_general(value, update, TN, preferred_element_type=F32)
        sdecay[h] = jnp.broadcast_to(jnp.exp(end), (8, wide))
        return carry

    lax.fori_loop(0, heads, local, 0)

    for d in range(1, nf):
        returned_arrived(d, 3)
        returned_arrived(d, 4)
    edge = rim.shape[1]

    def rim_copy(g):
        return remote(
            prev.at[g, SIGNAL, pl.ds(length - edge, edge), :], rim.at[g],
            ms.at[g], mr.at[g], sp=s + 1,
        )

    for g in range(nf):
        @pl.when(has_right)
        def _(g=g):
            rim_copy(g).start()

        @pl.when(s == 0)
        def _(g=g):
            rim[g] = jnp.zeros((edge, wide), BF)

    def state_copy(h):
        return remote(sout.at[h], sin.at[h], ss.at[h], sr.at[h], sp=s + 1)

    def chain(h, carry):
        @pl.when(has_left)
        def _():
            state_copy(h).wait_recv()

        @pl.when(s == 0)
        def _():
            sin[h] = jnp.zeros(sin.shape[1:], BF)

        @pl.when(has_right)
        def _():
            sout[h] = (sin[h].astype(F32) * sdecay[h, 0:1, :] + states[h]).astype(BF)
            state_copy(h).start()

        raw = inside[h] + lax.dot_general(reach[h], sin[h], NT, preferred_element_type=F32)
        scale = lax.rsqrt(jnp.mean(raw * raw, axis=-1, keepdims=True) + 1e-06)
        mix[1, :, pl.ds(pl.multiple_of(h * wide, wide), wide)] = (
            raw * scale * hgain[...]
        ).astype(BF)
        return carry

    out_arrived(1, 0)
    relay_out(1, 0, 2, 4).start()
    out_arrived(2, 1)
    relay_out(2, 1, 1, 5).start()
    lax.fori_loop(0, heads, chain, 0)

    for g in range(nf):
        @pl.when(has_left)
        def _(g=g):
            rim_copy(g).wait_recv()

    def conv(g, carry):
        padded = jnp.concatenate([rim[g], prev[g, SIGNAL]], axis=0).astype(F32)
        margin = taps.shape[1] - 1
        filtered = jnp.zeros((length, wide), F32)
        for o in range(margin + 1):
            start = edge - margin + o
            filtered = filtered + taps[g, o : o + 1, :] * padded[start : start + length]
        mix[0, :, pl.ds(pl.multiple_of(g * wide, wide), wide)] = (
            prev[g, GATE].astype(F32) * filtered
        ).astype(BF)
        return carry

    lax.fori_loop(0, nf, conv, 0)

    def partial(c, who):
        at = pl.ds(pl.multiple_of(who * half, half), half)
        return jnp.dot(mix[0, at, :], wo[c, 0], preferred_element_type=F32) + jnp.dot(
            mix[1, at, :], wo[c, 1], preferred_element_type=F32
        )

    def share(d):
        return remote(osend.at[d], orecv.at[d], es.at[d], er.at[d], tp=other)

    for j in range(2):
        pltpu.make_async_copy(outs[j], wo.at[f, j], oloc.at[j]).wait()
    cols = wo.shape[3]
    for d in range(nf):
        if d:
            for j in range(2):
                if (d, j) not in ((1, 0), (2, 1)):
                    out_arrived(d, j)
        c = f ^ d
        osend[d] = partial(c, other)
        share(d).start()
        at = pl.ds(pl.multiple_of(c * cols, cols), cols)
        mine = partial(c, t)
        share(d).wait_recv()
        out[0, :, at] = (mine + orecv[d]).astype(BF)

    for p in range(np_):
        def drained(b, carry, p=p):
            @pl.when(((b < s) & has_right) | ((b > s) & has_left))
            def _():
                relay(b, p, s).wait_send()

            return carry

        lax.fori_loop(0, ns, drained, 0)

        @pl.when(has_right)
        def _(p=p):
            own_right(p).wait_send()

        @pl.when(has_left)
        def _(p=p):
            own_left(p).wait_send()

        for d in range(1, nf):
            returned(d, p).wait_send()
    for d, j, to_d, slot in ((0, 0, 1, 0), (0, 1, 2, 1), (0, 1, 1, 2), (0, 0, 2, 3), (1, 0, 2, 4), (2, 1, 1, 5)):
        row_send(d, j, to_d, slot).wait_send()
        if d == 0:
            own_out(j, to_d, slot).wait_send()
        else:
            relay_out(d, j, to_d, slot).wait_send()
    for d in range(nf):
        twin(d).wait_send()
        share(d).wait_send()

    @pl.when(has_right)
    def _():
        for h in range(heads):
            state_copy(h).wait_send()
        for g in range(nf):
            rim_copy(g).wait_send()


def body(ns, nf, tokens, norm_gain, w0, w1, w2, w3, w4, conv_taps, floor_gate, leak, head_gain, cow, how):
    half, width = tokens.shape[1:]
    length = 2 * half
    heads = leak.shape[2]
    kd = w0.shape[0]
    wide = w0.shape[1] // nf
    assert heads == nf and nf == 4 and floor_gate.shape[0] == heads * wide
    taps = conv_taps.reshape(conv_taps.shape[0], nf, wide).transpose(1, 0, 2)
    vm = pl.BlockSpec(memory_space=pltpu.VMEM)
    dma = pltpu.SemaphoreType.DMA
    scratch = [
        pltpu.VMEM((nf, 2, half, width), BF),
        pltpu.VMEM((5, ns * kd, wide), BF),
        pltpu.VMEM((nf, 5, length, wide), BF),
        pltpu.VMEM((nf, 5, length, wide), BF),
        pltpu.VMEM((nf, 2) + cow.shape, BF),
        pltpu.VMEM((nf, 16, wide), BF),
        pltpu.VMEM((heads, length, wide), F32),
        pltpu.VMEM((heads, length, wide), BF),
        pltpu.VMEM((heads, wide, wide), F32),
        pltpu.VMEM((heads, 8, wide), F32),
        pltpu.VMEM((heads, wide, wide), BF),
        pltpu.VMEM((heads, wide, wide), BF),
        pltpu.VMEM((heads, length, wide), F32),
        pltpu.VMEM((heads, 8, length), F32),
        pltpu.VMEM((2, length, heads * wide), BF),
        pltpu.VMEM((nf, half, cow.shape[1]), F32),
        pltpu.VMEM((nf, half, cow.shape[1]), F32),
        dma((ns, 5)), dma((5,)), dma((ns, 5)), dma((5,)),
        dma((6,)), dma((nf, 2)), dma((nf,)), dma((nf,)),
        dma((nf, 5)), dma((nf, 5)),
        dma((6,)), dma((nf, 2)), dma((2,)),
        dma((nf,)), dma((nf,)), dma((heads,)), dma((heads,)),
        dma((nf,)), dma((nf,)),
    ]
    return pl.pallas_call(
        functools.partial(kernel, ns, nf),
        out_shape=jax.ShapeDtypeStruct(tokens.shape, BF),
        in_specs=[vm] * 14,
        out_specs=vm,
        scratch_shapes=scratch,
        compiler_params=pltpu.CompilerParams(
            collective_id=0, has_side_effects=True, vmem_limit_bytes=60 * 2**20
        ),
    )(
        tokens, norm_gain[None], w0, w1, w2, w3, w4, taps, floor_gate.reshape(heads, 1, wide),
        leak, leak[0].T, head_gain[None], cow, how,
    )


def solution(mesh):
    in_specs = (
        P("fs", ("sp", "tp"), None),
        P(),
        P("sp", "tp"),
        P("sp", "tp"),
        P("sp", "tp"),
        P("sp", "tp"),
        P("sp", "tp"),
        P(None, "tp"),
        P("tp"),
        P("fs", "sp", "tp"),
        P(),
        P("tp", "fs"),
        P("tp", "fs"),
    )
    out_specs = P("fs", ("sp", "tp"), None)
    step = functools.partial(body, mesh.shape["sp"], mesh.shape["fs"])
    return jax.shard_map(step, mesh=mesh, in_specs=in_specs, out_specs=out_specs, check_vma=False)
```

time: 290 us -> 109 us (0.38)
  Pallas kernels: 0 us -> 105 us
  blocking collectives: 101 us -> 0 us
  waiting for transfers between devices: 71 us -> 0 us
  matrix products: 47.2 us -> 0 us
  other arithmetic: 20.8 us -> 0 us
  starting transfers between devices: 20.1 us -> 0 us
  between operations: 13.8 us -> 0.01 us
  local copies, waits for them, and re-layouts: 15.3 us -> 3.6 us
    pallas_call x0 -> x1, Pallas kernels: none -> 105 us  [body(): pl.pallas_call(functools.partial(kernel, ns, nf), out_shape=jax.ShapeDtyp...]
    all_gather x6 -> x0, blocking collectives: 101 us -> none  [the longest x5 88.6 us: body(): lax.all_gather(part, 'sp', axis=0, tiled=True)]
    dot_general x32 -> x0, matrix products: 47.2 us -> none  [the longest x5 22.8 us: body(): jnp.dot(flat_rows, piece, preferred_element_type=jnp.float32)]
    all_gather x5 -> x0, waiting for transfers between devices: 44.4 us -> none  [the longest x1 22.2 us: body(): pooled = lax.all_gather(normed[None], 'fs', axis=0, tiled=True)]
    all_to_all x5 -> x0, starting transfers between devices: 17.7 us -> none  [body(): lax.all_to_all(as_sent(quarters), 'fs', split_axis=0, concat_axis=2, tile...]
    all_to_all x5 -> x0, waiting for transfers between devices: 14 us -> none  [body(): lax.all_to_all(as_sent(quarters), 'fs', split_axis=0, concat_axis=2, tile...]
    reduce_scatter x1 -> x0, waiting for transfers between devices: 11.3 us -> none  [body(): lax.psum_scatter(jnp.dot(conv_mix, conv_full, preferred_element_type=jnp....]
    squeeze x6 -> x0, local copies, waits for them, and re-layouts: 5.52 us -> none  [block_chain(): lax.scan(advance, initial, (split_blocks(query), split_blocks(keys), spli...]
  transfers between devices with their start and end apart: 12 -> 0, of which waited for: 9 -> 0; matrix products, arithmetic and copies ran while one was open for 24% -> 0% of each run, Pallas kernels for 0% -> 0%
where the time goes in v1:
time: 109 us; the launch traced here: 108 us
  Pallas kernels  105 us (96%)
  local copies, waits for them, and re-layouts  3.6 us (3%)
    pallas_call x1, Pallas kernels, body(): pl.pallas_call(functools.partial(kernel, ns, nf), out_shape=jax.ShapeDtyp...  105 us
    unnamed x4, local copies, waits for them, and re-layouts  3.6 us

profile of v1, /device:TPU:0, one launch (start us, length us, event | category | flops | bytes accessed | tf_op | source)
XLA Modules:
  0.0 108.3 jit_solution(16840011224210173869)
XLA Ops:
  0.0 0.0 copy-start
  0.0 0.7 copy-done
  0.7 0.8 copy.14.leak
  1.5 104.7 %shard_map.127 = bf16[1,192,2048]{2,1,0:T(8,128)(2,1)} custom-call(bf16[1,192,2048]{2,1,0:T(8,128)(2,1)} %tok.1, f32[1,2048]{1,0:T(1,128)} %bitcast.10, bf16[512,512]{1,0:T(8,128)(2,1)} %w0.1, bf16[512,512]{1,0:T(8,128)(2,1)} %w1.1, bf16[512,512]{1,0:T(8,128)(2,1)} %w2.1, bf16[512,512]{1,0:T(8,128)(2,1)} %w3.1, bf16[512,512]{1,0:T(8,128)(2,1)} %w4.1, ...), custom_call_target="tpu_custom_call" | custom-call | tf_op jit(solution)/shard_map/pallas_call | solution.py:422
  106.2 2.1 %copy.16 = bf16[1,192,2048]{2,1,0:T(8,128)(2,1)} copy(bf16[1,192,2048]{2,1,0:T(8,128)(2,1)} %shard_map.127) | data formatting | bytes 1572864
Async XLA Ops:
  0.0 0.7 copy-start

commit v2 on v1

--- a/solution.py
+++ b/solution.py
@@ -20,8 +20,8 @@
     tok, gain, w0, w1, w2, w3, w4, taps, floor, leak, leak_t, hgain, cow, how,
     out,
     rows, wg, psend, prev, wo, rim, inside, reach, states, sdecay, sin, sout,
-    lcol, lrow, mix, osend, orecv,
-    zs, zsl, zr, zloc, rs, rr, ts, tr, ps, pr, os_, or_, oloc, ms, mr, ss, sr, es, er,
+    lcol, lrow, mix, osend, orecv, through,
+    zs, zsl, zr, zloc, rs, rr, ts, tr, ps, pr, os_, or_, oloc, ms, mr, ss, sr, es, er, ds, dr, ns_, nr,
 ):
     s, f, t = lax.axis_index("sp"), lax.axis_index("fs"), lax.axis_index("tp")
     other = 1 - t
@@ -112,15 +112,17 @@
     x = tok[0].astype(F32)
     center = x - jnp.mean(x, axis=-1, keepdims=True)
     spread = jnp.mean(center * center, axis=-1, keepdims=True)
-    rows[f, t] = (center * lax.rsqrt(spread + 1e-05) * gain[...]).astype(BF)
+    rows[f, pl.ds(pl.multiple_of(t * half, half), half), :] = (
+        center * lax.rsqrt(spread + 1e-05) * gain[...]
+    ).astype(BF)
 
     quarter = half // 2
 
     def piece(g, j):
-        return rows.at[g, t, pl.ds(j * quarter, quarter), :]
-
-    def row_copy(g, j, to, slot):
-        return remote(piece(g, j), piece(g, j), rs.at[slot], rr.at[g ^ f ^ to, j], fs=to)
+        return rows.at[g, pl.ds(pl.multiple_of(t * half + j * quarter, quarter), quarter), :]
+
+    def core_rows(g, core):
+        return rows.at[g, pl.ds(pl.multiple_of(core * half, half), half), :]
 
     def row_arrived(d, j):
         g = f ^ d
@@ -133,11 +135,11 @@
 
     def twin(d):
         g = f ^ d
-        return remote(rows.at[g, t], rows.at[g, t], ts.at[d], tr.at[d], tp=other)
+        return remote(core_rows(g, t), core_rows(g, t), ts.at[d], tr.at[d], tp=other)
 
     def twin_arrived(d):
         g = f ^ d
-        remote(rows.at[g, other], rows.at[g, other], ts.at[d], tr.at[d], tp=other).wait_recv()
+        remote(core_rows(g, other), core_rows(g, other), ts.at[d], tr.at[d], tp=other).wait_recv()
 
     row_send(0, 0, 1, 0).start()
     row_send(0, 1, 2, 1).start()
@@ -157,11 +159,29 @@
         lcol[h] = jnp.broadcast_to(lsum[:, h : h + 1], (length, wide))
         lrow[h] = jnp.broadcast_to(lsum_t[h : h + 1, :], (8, length))
 
+    outs = (cow, how)
+
+    def own_out(j, to_d, slot):
+        return remote(outs[j], wo.at[f, j], os_.at[slot], or_.at[to_d, j], fs=f ^ to_d)
+
+    def relay_out(d, j, to_d, slot):
+        g = f ^ d
+        return remote(wo.at[g, j], wo.at[g, j], os_.at[slot], or_.at[d ^ to_d, j], fs=f ^ to_d)
+
+    def out_arrived(d, j):
+        g = f ^ d
+        remote(wo.at[g, j], wo.at[g, j], os_.at[0], or_.at[d, j], fs=f ^ 1).wait_recv()
+
+    for j in range(2):
+        pltpu.make_async_copy(outs[j], wo.at[f, j], oloc.at[j]).start()
+
     zrelay(0)
     row_arrived(1, 0)
     row_send(1, 0, 2, 4).start()
     row_arrived(2, 1)
     row_send(2, 1, 1, 5).start()
+    own_out(0, 1, 0).start()
+    own_out(1, 2, 1).start()
     zrelay(1)
     row_arrived(1, 1)
     twin(1).start()
@@ -176,8 +196,7 @@
 
     def project(p):
         def one(g, carry):
-            lhs = jnp.concatenate([rows[g, 0], rows[g, 1]], axis=0)
-            psend[g, p] = jnp.dot(lhs, wg[p], preferred_element_type=F32).astype(BF)
+            psend[g, p] = jnp.dot(rows[g], wg[p], preferred_element_type=F32).astype(BF)
             return carry
 
         lax.fori_loop(0, nf, one, 0)
@@ -193,45 +212,41 @@
         g = f ^ d
         remote(psend.at[g, p], prev.at[g, p], ps.at[d, p], pr.at[d, p], fs=g).wait_recv()
 
+    def gathered(p):
+        for d in range(1, nf):
+            returned_arrived(d, p)
+
     project(0)
     project(1)
     project(2)
+    own_out(1, 1, 2).start()
+    own_out(0, 2, 3).start()
     zrelay(3)
     project(3)
     zrelay(4)
     project(4)
-
-    outs = (cow, how)
-
-    def own_out(j, to_d, slot):
-        return remote(outs[j], wo.at[f, j], os_.at[slot], or_.at[to_d, j], fs=f ^ to_d)
-
-    def relay_out(d, j, to_d, slot):
-        g = f ^ d
-        return remote(wo.at[g, j], wo.at[g, j], os_.at[slot], or_.at[d ^ to_d, j], fs=f ^ to_d)
-
-    def out_arrived(d, j):
-        g = f ^ d
-        remote(wo.at[g, j], wo.at[g, j], os_.at[0], or_.at[d, j], fs=f ^ 1).wait_recv()
-
-    own_out(0, 1, 0).start()
-    own_out(1, 2, 1).start()
-    own_out(1, 1, 2).start()
-    own_out(0, 2, 3).start()
-    for j in range(2):
-        pltpu.make_async_copy(outs[j], wo.at[f, j], oloc.at[j]).start()
+    out_arrived(1, 0)
+    relay_out(1, 0, 2, 4).start()
+    out_arrived(2, 1)
+    relay_out(2, 1, 1, 5).start()
 
     for p in range(3):
-        for d in range(1, nf):
-            returned_arrived(d, p)
+        gathered(p)
     causal = ri >= ci
+    tril_short = tril.astype(BF)
 
     def local(h, carry):
         fl = floor[h]
         logits = prev[h, FORGET].astype(F32)
         retain = fl + (1.0 - fl) * jax.nn.sigmoid(logits)
         keys = (1.0 - fl) * jax.nn.sigmoid(-logits)
-        total = jnp.dot(tril, jnp.log(retain), precision=high, preferred_element_type=F32)
+        step = jnp.log(retain)
+        coarse = step.astype(BF)
+        fine = (step - coarse.astype(F32)).astype(BF)
+        both = jnp.dot(
+            tril_short, jnp.concatenate([coarse, fine], axis=1), preferred_element_type=F32
+        )
+        total = both[:, :wide] + both[:, wide:]
         raw = prev[h, QUERY].astype(F32)
         query = raw * jax.nn.sigmoid(raw) * jnp.exp(total)
         value = prev[h, VALUE]
@@ -252,9 +267,7 @@
 
     lax.fori_loop(0, heads, local, 0)
 
-    for d in range(1, nf):
-        returned_arrived(d, 3)
-        returned_arrived(d, 4)
+    gathered(3)
     edge = rim.shape[1]
 
     def rim_copy(g):
@@ -296,11 +309,8 @@
         ).astype(BF)
         return carry
 
-    out_arrived(1, 0)
-    relay_out(1, 0, 2, 4).start()
-    out_arrived(2, 1)
-    relay_out(2, 1, 1, 5).start()
     lax.fori_loop(0, heads, chain, 0)
+    gathered(4)
 
     for g in range(nf):
         @pl.when(has_left)
@@ -395,7 +405,7 @@
     vm = pl.BlockSpec(memory_space=pltpu.VMEM)
     dma = pltpu.SemaphoreType.DMA
     scratch = [
-        pltpu.VMEM((nf, 2, half, width), BF),
+        pltpu.VMEM((nf, length, width), BF),
         pltpu.VMEM((5, ns * kd, wide), BF),
         pltpu.VMEM((nf, 5, length, wide), BF),
         pltpu.VMEM((nf, 5, length, wide), BF),
@@ -412,12 +422,14 @@
         pltpu.VMEM((2, length, heads * wide), BF),
         pltpu.VMEM((nf, half, cow.shape[1]), F32),
         pltpu.VMEM((nf, half, cow.shape[1]), F32),
+        pltpu.VMEM((2, 5, half, wide), BF),
         dma((ns, 5)), dma((5,)), dma((ns, 5)), dma((5,)),
         dma((6,)), dma((nf, 2)), dma((nf,)), dma((nf,)),
         dma((nf, 5)), dma((nf, 5)),
         dma((6,)), dma((nf, 2)), dma((2,)),
         dma((nf,)), dma((nf,)), dma((heads,)), dma((heads,)),
         dma((nf,)), dma((nf,)),
+        dma((2, 5)), dma((2, 5)), dma((2, 5)), dma((2, 5)),
     ]
     return pl.pallas_call(
         functools.partial(kernel, ns, nf),

time: 109 us -> 96 us (0.88)
  Pallas kernels: 105 us -> 92.2 us
    pallas_call x1, Pallas kernels: 105 us -> 92.2 us  [body(): pl.pallas_call(functools.partial(kernel, ns, nf), out_shape=jax.ShapeDtyp...]
where the time goes in v2:
time: 96 us; the launch traced here: 95.8 us
  Pallas kernels  92.2 us (96%)
  local copies, waits for them, and re-layouts  3.6 us (4%)
    pallas_call x1, Pallas kernels, body(): pl.pallas_call(functools.partial(kernel, ns, nf), out_shape=jax.ShapeDtyp...  92.2 us
    unnamed x4, local copies, waits for them, and re-layouts  3.6 us

profile of v2, /device:TPU:0, one launch (start us, length us, event | category | flops | bytes accessed | tf_op | source)
XLA Modules:
  0.0 95.8 jit_solution(16257246778117559449)
XLA Ops:
  0.0 0.0 copy-start
  0.0 0.7 copy-done
  0.7 0.8 copy.14.leak
  1.5 92.2 %shard_map.127 = bf16[1,192,2048]{2,1,0:T(8,128)(2,1)} custom-call(bf16[1,192,2048]{2,1,0:T(8,128)(2,1)} %tok.1, f32[1,2048]{1,0:T(1,128)} %bitcast.10, bf16[512,512]{1,0:T(8,128)(2,1)} %w0.1, bf16[512,512]{1,0:T(8,128)(2,1)} %w1.1, bf16[512,512]{1,0:T(8,128)(2,1)} %w2.1, bf16[512,512]{1,0:T(8,128)(2,1)} %w3.1, bf16[512,512]{1,0:T(8,128)(2,1)} %w4.1, ...), custom_call_target="tpu_custom_call" | custom-call | tf_op jit(solution)/shard_map/pallas_call | solution.py:434
  93.8 2.1 %copy.16 = bf16[1,192,2048]{2,1,0:T(8,128)(2,1)} copy(bf16[1,192,2048]{2,1,0:T(8,128)(2,1)} %shard_map.127) | data formatting | bytes 1572864
Async XLA Ops:
  0.0 0.7 copy-start
